TPU v7x, 32 devices: a whole 2x2x4 slice. The times are simulated.
32 devices in a mesh: sp: 8 (over z, x), dp: 4 (over y, core).
Axes of the slice: x: 2, y: 2, z: 4, core: 2. Of those that a mesh axis runs over, the one named last changes fastest.
Arguments:
- stream: bfloat16 [4, 1536, 2048], P('dp', 'sp'), may hold values from -6 to 6
- queries: bfloat16 [4, 1536, 2048], P('dp', 'sp'), may hold values from -6 to 6
- key_rows: bfloat16 [4, 1536, 2048], P('dp', 'sp'), may hold values from -6 to 6
- value_rows: bfloat16 [4, 1536, 4096], P('dp', 'sp'), may hold values from -6 to 6
- input_gate: bfloat16 [4, 1536, 16], P('dp', 'sp'), may hold values from -4 to 206
- forget_gate: bfloat16 [4, 1536, 16], P('dp', 'sp'), may hold values from 0 to 12
- head_gain: float32 [16, 256], P('sp'), may hold values from 0.1 to 1.9
- out_weight: bfloat16 [4096, 2048], P('sp'), may hold values from -0.09375 to 0.09375
- mix_gain: float32 [2048], replicated, may hold values from 0.1 to 1.9
- ffn_gain: float32 [2048], replicated, may hold values from 0.1 to 1.9
- final_gain: float32 [2048], replicated, may hold values from 0.1 to 1.9
- expert_ids: int32 [4, 1536, 4], P('dp', 'sp'), may hold values from 0 to 31, all different within a row; in each aligned block of 192 rows (0 to 191, 192 to 383, ..., all dimensions but the last counted through in order) at most 36 rows name the same one
- route_scores: float32 [4, 1536, 4], P('dp', 'sp'), may hold values from 0.05 to 1
- expert_gate: bfloat16 [32, 2048, 512], P(('sp', 'dp')), may hold values from -0.125 to 0.125
- expert_up: bfloat16 [32, 2048, 512], P(('sp', 'dp')), may hold values from -0.125 to 0.125
- expert_down: bfloat16 [32, 512, 2048], P(('sp', 'dp')), may hold values from -0.25 to 0.25
- shared_gate: bfloat16 [2048, 512], replicated, may hold values from -0.125 to 0.125
- shared_up: bfloat16 [2048, 512], replicated, may hold values from -0.125 to 0.125
- shared_down: bfloat16 [512, 2048], replicated, may hold values from -0.25 to 0.25
Outputs:
- updated: bfloat16 [4, 1536, 2048], P('dp', 'sp')
Inputs may be any that keep to these rules, and one draw needn't show every extreme that they name: `expert_ids`: each token names 4 different experts. Among the tokens of one device no expert is named by more than 36 tokens, a bound that some block reaches of some device.
All inputs are finite; a program needn't handle non-finite values.
Results may differ from a plain program's by a relative error of at most 0.006.
Values may be sent and summed in bfloat16 or wider, within the bound.
No kernel may reach another device: no remote copies, remote signals or barrier semaphores. Data moves between devices by JAX's collectives and lax.ppermute only.
A program may use at most 128 MiB of HBM per device.

v0:
```python
import jax
import jax.numpy as jnp
from jax import lax
from jax.sharding import PartitionSpec as P

BLOCK = 256


EPSILON = 1e-06
ROUTE_BOOST = 2.5
HIGHEST = lax.Precision.HIGHEST


def root_norm(values, gains):
    return values * lax.rsqrt(jnp.mean(values * values, axis=-1, keepdims=True) + EPSILON) * gains


def cell_block(carry, pieces):
    state, normal, stabilizer = carry
    query_part, key_part, value_part, gate_part, decay_part = pieces
    length = query_part.shape[1]
    causal = jnp.tril(jnp.ones((length, length), dtype=bool))
    cumulative = jnp.cumsum(decay_part, axis=-1)
    logits = jnp.where(
        causal[None],
        cumulative[:, :, None] - cumulative[:, None, :] + gate_part[:, None, :],
        -jnp.inf,
    )
    peak = jnp.maximum(cumulative + stabilizer[:, None], jnp.max(logits, axis=-1))
    weights = jnp.exp(logits - peak[:, :, None])
    scores = jnp.einsum("hld,hsd->hls", query_part, key_part, precision=HIGHEST) * weights
    carried = jnp.exp(cumulative + stabilizer[:, None] - peak)
    numerator = jnp.einsum("hls,hsv->hlv", scores, value_part, precision=HIGHEST) + carried[
        :, :, None
    ] * jnp.einsum("hvd,hld->hlv", state, query_part, precision=HIGHEST)
    denominator = jnp.sum(scores, axis=-1) + carried * jnp.einsum(
        "hd,hld->hl", normal, query_part, precision=HIGHEST
    )
    result = numerator / jnp.maximum(jnp.abs(denominator), jnp.exp(-peak))[:, :, None]
    block_end = cumulative[:, -1]
    write_log = block_end[:, None] - cumulative + gate_part
    peak_next = jnp.maximum(block_end + stabilizer, jnp.max(write_log, axis=-1))
    decay_all = jnp.exp(block_end + stabilizer - peak_next)
    written = jnp.exp(write_log - peak_next[:, None])[:, :, None] * key_part
    state = decay_all[:, None, None] * state + jnp.einsum(
        "hlv,hld->hvd", value_part, written, precision=HIGHEST
    )
    normal = decay_all[:, None] * normal + jnp.sum(written, axis=1)
    return ((state, normal, peak_next), result)


def memory_cell(queries, key_rows, value_rows, input_gate, forget_gate):
    length, head_count = (queries.shape[0], queries.shape[1])
    key_width = queries.shape[2]
    value_width = value_rows.shape[2]
    blocks = length // BLOCK

    def to_blocks(tensor):
        shaped = tensor.astype(jnp.float32).reshape((blocks, BLOCK, head_count) + tensor.shape[2:])
        return jnp.moveaxis(shaped, 2, 1)

    decay_log = jax.nn.log_sigmoid(forget_gate.astype(jnp.float32))
    start_state = (
        jnp.zeros((head_count, value_width, key_width), jnp.float32),
        jnp.zeros((head_count, key_width), jnp.float32),
        jnp.zeros((head_count,), jnp.float32),
    )
    pieces = (
        to_blocks(queries),
        to_blocks(key_rows) * key_width ** (-0.5),
        to_blocks(value_rows),
        to_blocks(input_gate),
        to_blocks(decay_log),
    )
    _, outputs = lax.scan(cell_block, start_state, pieces)
    return jnp.moveaxis(outputs, 1, 2).reshape(length, head_count, value_width)


def local(
    stream,
    queries,
    key_rows,
    value_rows,
    input_gate,
    forget_gate,
    head_gain,
    out_weight,
    mix_gain,
    ffn_gain,
    final_gain,
    expert_ids,
    route_scores,
    expert_gate,
    expert_up,
    expert_down,
    shared_gate,
    shared_up,
    shared_down,
):
    token_count = stream.shape[1]
    model_width = stream.shape[2]
    head_count = head_gain.shape[0]
    value_width = head_gain.shape[1]
    head_queries, head_keys, head_values, head_input, head_forget = (
        lax.all_to_all(queries, "sp", split_axis=2, concat_axis=1, tiled=True),
        lax.all_to_all(key_rows, "sp", split_axis=2, concat_axis=1, tiled=True),
        lax.all_to_all(value_rows, "sp", split_axis=2, concat_axis=1, tiled=True),
        lax.all_to_all(input_gate, "sp", split_axis=2, concat_axis=1, tiled=True),
        lax.all_to_all(forget_gate, "sp", split_axis=2, concat_axis=1, tiled=True),
    )
    length = head_input.shape[1]
    cell_out = memory_cell(
        head_queries[0].reshape(length, head_count, -1),
        head_keys[0].reshape(length, head_count, -1),
        head_values[0].reshape(length, head_count, value_width),
        head_input[0],
        head_forget[0],
    )
    normed = (
        root_norm(cell_out, head_gain)
        .astype(jnp.bfloat16)
        .reshape(1, length, head_count * value_width)
    )
    token_rows = lax.all_to_all(normed, "sp", split_axis=1, concat_axis=2, tiled=True)[0]
    mixer_out = jnp.dot(
        token_rows,
        lax.all_gather(out_weight, "sp", axis=0, tiled=True),
        preferred_element_type=jnp.float32,
    )
    residual = stream[0].astype(jnp.float32) + root_norm(mixer_out, mix_gain)
    ffn_input = root_norm(residual, ffn_gain).astype(jnp.bfloat16)
    top_count = expert_ids.shape[2]
    local_count = expert_gate.shape[0]
    expert_count = lax.axis_size("sp") * lax.axis_size("dp") * local_count
    capacity = max(2, 3 * token_count * top_count // (2 * expert_count))
    route_ids = expert_ids[0].reshape(-1)
    chosen = (route_ids[:, None] == jnp.arange(expert_count, dtype=jnp.int32)[None, :]).astype(
        jnp.int32
    )
    before = jnp.sum((jnp.cumsum(chosen, axis=0) - chosen) * chosen, axis=1)
    slot_index = route_ids * capacity + before
    slot_owner = jnp.full((expert_count * capacity,), -1, jnp.int32)
    slot_owner = slot_owner.at[slot_index].set(jnp.arange(token_count * top_count, dtype=jnp.int32))
    filled = slot_owner >= 0
    source = jnp.where(filled, slot_owner // top_count, 0)
    outgoing = jnp.where(filled[:, None], ffn_input[source], jnp.zeros((), jnp.bfloat16))
    outgoing = outgoing.reshape(expert_count, capacity, model_width)
    slot_rows = lax.all_to_all(outgoing, ("sp", "dp"), split_axis=0, concat_axis=0, tiled=True)
    shaped = slot_rows.reshape(-1, local_count, slot_rows.shape[1], model_width)
    gate_proj = jnp.einsum(
        "nlcd,ldf->nlcf", shaped, expert_gate, preferred_element_type=jnp.float32
    )
    up_proj = jnp.einsum("nlcd,ldf->nlcf", shaped, expert_up, preferred_element_type=jnp.float32)
    hidden = (jax.nn.silu(gate_proj) * up_proj).astype(jnp.bfloat16)
    answer = jnp.einsum("nlcf,lfd->nlcd", hidden, expert_down, preferred_element_type=jnp.float32)
    expert_out = answer.astype(jnp.bfloat16).reshape(slot_rows.shape)
    returned = lax.all_to_all(expert_out, ("sp", "dp"), split_axis=0, concat_axis=0, tiled=True)
    answers = returned.reshape(expert_count * capacity, model_width)[slot_index]
    answers = answers.reshape(token_count, top_count, model_width)
    scores = route_scores[0]
    route_share = scores / jnp.sum(scores, axis=1, keepdims=True) * ROUTE_BOOST
    routed = jnp.zeros((token_count, model_width), jnp.float32)
    for column in range(top_count):
        routed = routed + route_share[:, column][:, None] * answers[:, column].astype(jnp.float32)
    shared_hidden = (
        jax.nn.silu(jnp.dot(ffn_input, shared_gate, preferred_element_type=jnp.float32))
        * jnp.dot(ffn_input, shared_up, preferred_element_type=jnp.float32)
    ).astype(jnp.bfloat16)
    shared_out = jnp.dot(shared_hidden, shared_down, preferred_element_type=jnp.float32)
    moe_total = routed + shared_out
    result = (residual + root_norm(moe_total, final_gain)).astype(jnp.bfloat16)
    return result[None]


def solution(mesh):
    placed = (
        P("dp", "sp", None),
        P("dp", "sp", None),
        P("dp", "sp", None),
        P("dp", "sp", None),
        P("dp", "sp", None),
        P("dp", "sp", None),
        P("sp", None),
        P("sp", None),
        P(),
        P(),
        P(),
        P("dp", "sp", None),
        P("dp", "sp", None),
        P(("sp", "dp"), None, None),
        P(("sp", "dp"), None, None),
        P(("sp", "dp"), None, None),
        P(),
        P(),
        P(),
    )
    return jax.shard_map(
        local, mesh=mesh, in_specs=placed, out_specs=P("dp", "sp", None), check_vma=False
    )
```

profile of v0, /device:TPU:0, one launch (start us, length us, event | category | flops | bytes accessed | tf_op | source)
XLA Modules:
  0.0 747.5 jit_solution(1196723427909744174)
XLA Ops:
  9.1 7.3 all-to-all-start
  18.3 4.6 all-to-all-done
  22.9 3.3 all-to-all-start.1
  26.2 5.9 copy.84
  32.1 12.6 %reduce.11 = bf16[2048,192]{1,0:T(8,128)(2,1)S(1)} reduce(bf16[2048,1,192]{2,1,0:T(2,128)(2,1)} %bitcast.311, bf16[]{:T(256)} %broadcast.272), dimensions={1}, to_apply=%bitcast.222.reduce_sub_computation | reduce | bytes 1572866
  46.8 6.1 all-to-all-start.3
  52.8 3.8 copy.86
  56.6 12.6 %reduce.12 = bf16[2048,192]{1,0:T(8,128)(2,1)S(1)} reduce(bf16[2048,1,192]{2,1,0:T(2,128)(2,1)} %bitcast.312, bf16[]{:T(256)} %broadcast.272), dimensions={1}, to_apply=%bitcast.216.reduce_sub_computation | reduce | bytes 1572866
  71.5 5.7 all-to-all-start.4
  77.9 9.9 %copy.82 = bf16[1,192,4096]{1,0,2:T(2,128)(2,1)} copy(bf16[1,192,4096]{2,1,0:T(8,128)(2,1)} %param.24) | data formatting | bytes 3145728 | tf_op args[3]
  87.9 25.0 %reduce.10 = bf16[4096,192]{1,0:T(8,128)(2,1)} reduce(bf16[4096,1,192]{2,1,0:T(2,128)(2,1)} %bitcast.303, bf16[]{:T(256)} %broadcast.272), dimensions={1}, to_apply=%bitcast.214.reduce_sub_computation | reduce | bytes 3145730
  112.8 6.7 reshape.420
  119.5 6.1 all-to-all-start.2
  126.0 5.9 reshape.429
  131.9 5.3 convert_multiply_fusion
  137.2 5.9 copy.85
  143.1 2.9 mul.234
  146.0 3.7 reshape.423
  149.7 5.9 copy.87
  155.6 3.0 reshape.379
  158.6 38.3 %all-to-all-done.2 = bf16[8,2,49152]{2,1,0:T(2,128)(2,1)} async-done(((bf16[8,2,49152]{2,1,0:T(2,128)(2,1)}), bf16[8,2,49152]{2,1,0:T(2,128)(2,1)}, u32[]{:S(2)}, u32[]{:S(2)}) %all-to-all-start.2) | async-done | bytes 1572896 | tf_op jit(solution)/shard_map/all_to_all | solution.py:107
  196.9 7.2 reshape.421
  204.1 10.8 %copy.83 = f32[1,192,8,512]{3,1,2,0:T(8,128)} copy(bf16[1,192,8,512]{1,0,3,2:T(2,128)(2,1)} %bitcast.302) | data formatting | bytes 4718592 | tf_op jit(solution)/shard_map/transpose | solution.py:60
  215.0 5.2 reshape.378
  220.2 82.9 %while.17 = (s32[]{:T(128)}, f32[2,256,128]{2,1,0:T(8,128)}, f32[2,128]{1,0:T(2,128)S(1)}, f32[2]{0:T(128)S(1)}, f32[6,2,256,256]{3,2,1,0:T(8,128)}, /*index=5*/...) while((s32[]{:T(128)}, f32[2,256,128]{2,1,0:T(8,128)}, ...), condition=%wide.region_7.8_spmd.clone, body=%wide.region_0.7_spmd.clone.sunk | while | flops 1009719296 | bytes 9456510 | solution.py:75
  228.0 3.0 fusion.103
  241.2 3.0 fusion.103
  244.2 2.3 convolution_add_fusion.4
  251.5 2.3 convolution_multiply_fusion.4
  255.3 3.0 fusion.103
  269.4 3.0 fusion.103
  272.4 2.3 convolution_add_fusion.4
  283.5 3.0 fusion.103
  293.9 2.3 convolution_multiply_fusion.4
  297.7 3.0 fusion.103
  303.1 2.4 multiply_reduce_fusion
  305.8 3.2 mul.237
  308.9 5.6 mul.238
  314.6 6.0 copy.93
  320.6 5.5 reshape.364
  326.1 3.7 multiply_convert_fusion
  329.8 14.1 %copy.176 = bf16[1,1536,512]{2,0,1:T(2,128)(2,1)} copy(bf16[1,1536,512]{2,1,0:T(8,128)(2,1)S(1)} %multiply_convert_fusion) | data formatting | bytes 3145728 | tf_op jit(solution)/shard_map/convert_element_type | solution.py:121
  343.9 12.0 %reduce.13 = bf16[1536,512]{1,0:T(8,128)(2,1)} reduce(bf16[1536,1,512]{2,1,0:T(2,128)(2,1)} %bitcast.306, bf16[]{:T(256)} %broadcast.272), dimensions={1}, to_apply=%bitcast.255.reduce_sub_computation | reduce | bytes 3145730
  356.0 4.1 reshape.430
  360.1 4.4 all-to-all-start.5
  367.3 3.4 scatter_custom_fusion
  370.9 28.7 %all-to-all-done.5 = bf16[8,2,49152]{2,1,0:T(2,128)(2,1)} async-done(((bf16[8,2,49152]{2,1,0:T(2,128)(2,1)}), bf16[8,2,49152]{2,1,0:T(2,128)(2,1)}, u32[]{:S(2)}, u32[]{:S(2)}) %all-to-all-start.5) | async-done | bytes 1572896 | tf_op jit(solution)/shard_map/all_to_all | solution.py:124
  399.6 6.5 reshape.431
  409.8 8.2 %multiply_reduce_fusion.3 = (f32[192]{0:T(256)S(1)}, f32[192,2048]{1,0:T(8,128)S(1)}) fusion(bf16[192,4096]{1,0:T(8,128)(2,1)} %bitcast.318, bf16[4096,2048]{1,0:T(8,128)(2,1)} %all-gather.2.cloned.1.call-done), kind=kOutput, calls=%fused_computation.78 | convolution fusion | flops 3222011648 | bytes 19923712 | tf_op jit(solution)/shard_map/dot_general | solution.py:125
  419.6 6.0 gather_fusion
  425.6 7.2 gather.9
  432.8 2.9 broadcast_select_fusion.2
  435.7 119.3 %all_to_all.70 = bf16[32,36,2048]{2,1,0:T(8,128)(2,1)S(1)} all-to-all(bf16[32,36,2048]{2,1,0:T(8,128)(2,1)S(1)} %broadcast_select_fusion.2), channel_id=1, replica_groups=mesh['sp'=8,'dp'=4] {'sp','dp'}, dimensions={0} | all-to-all | bytes 9437184 | tf_op jit(solution)/shard_map/all_to_all | solution.py:148
  555.1 2.3 copy-done.3
  557.4 4.5 fusion.24
  561.9 10.5 %convolution_convert_fusion = bf16[32,36,2048]{2,1,0:T(8,128)(2,1)} fusion(bf16[1,512,2048]{2,1,0:T(8,128)(2,1)S(1)} %copy-done, f32[32,36,512]{2,1,0:T(8,128)} %fusion.24, bf16[32,36,2048]{2,1,0:T(8,128)(2,1)} %copy-done.3, bf16[1,2048,512]{2,1,0:T(8,128)(2,1)} %param.34), kind=kOutput, calls=%fused_computation.49 | convolution fusion | flops 4837736448 | bytes 15990784 | tf_op jit(solution)/shard_map/nlcf,lfd->nlcd/dot_general | solution.py:155
  572.4 4.1 all-to-all-start.7
  578.8 114.7 %all-to-all-done.7 = bf16[32,36,2048]{2,1,0:T(8,128)(2,1)} async-done(((bf16[32,36,2048]{2,1,0:T(8,128)(2,1)}), bf16[32,36,2048]{2,1,0:T(8,128)(2,1)}, u32[]{:S(2)}, u32[]{:S(2)}) %all-to-all-start.7) | async-done | bytes 4718624 | tf_op jit(solution)/shard_map/all_to_all | solution.py:157
  693.5 7.2 reshape.370
  700.7 10.0 %gather_fusion.1 = bf16[768,2048]{1,0:T(8,128)(2,1)} fusion(bf16[1152,2048]{1,0:T(8,128)(2,1)} %reshape.370, s32[1024]{0:T(1024)S(1)} %pad_clamp_fusion.1), kind=kCustom, calls=%fused_computation.1 | custom fusion | bytes 6294528 | tf_op jit(solution)/shard_map/gather | solution.py:158
  710.8 5.7 reshape.371
  716.5 12.3 %fusion.64 = (bf16[192,1,2048]{2,1,0:T(2,128)(2,1)}, bf16[192,1,2048]{2,1,0:T(2,128)(2,1)}, bf16[192,1,2048]{2,1,0:T(2,128)(2,1)}, bf16[192,1,2048]{2,1,0:T(2,128)(2,1)}) fusion(bf16[192,4,2048]{2,1,0:T(4,128)(2,1)} %reshape.371), kind=kLoop, calls=%fused_computation.135 | loop fusion | bytes 6291456 | tf_op jit(solution)/shard_map/slice | solution.py:164
  728.8 8.0 %multiply_reduce_fusion.1 = (f32[192]{0:T(256)S(1)}, f32[192,2048]{1,0:T(8,128)}) fusion(bf16[512,2048]{1,0:T(8,128)(2,1)} %param.39, bf16[192,2048]{1,0:T(8,128)(2,1)S(1)} %multiply_convert_fusion.1, bf16[2048,512]{1,0:T(8,128)(2,1)} %param.38, f32[192,512]{1,0:T(8,128)S(1)} %fusion.66, bf16[192,1,2048]{2,1,0:T(2,128)(2,1)} %get-tuple-element.159, ...), kind=kOutput, calls=%fused_computation.75 | convolution fusion | flops 811401024 | bytes 10096384 | tf_op jit(solution)/shard_map/dot_general | solution.py:169
  736.8 3.4 fusion.37
  (228 shorter events, 75.6 us)
Async XLA Ops:
  6.5 555.3 %copy-start = (bf16[1,512,2048]{2,1,0:T(8,128)(2,1)S(1)}, bf16[1,512,2048]{2,1,0:T(8,128)(2,1)}, u32[]{:S(2)}) copy-start(bf16[1,512,2048]{2,1,0:T(8,128)(2,1)} %param.36) | copy-start | bytes 6291460
  9.1 13.8 %all-to-all-start = ((bf16[8,2,192]{2,1,0:T(2,128)(2,1)}), bf16[8,2,192]{2,1,0:T(2,128)(2,1)S(1)}, u32[]{:S(2)}, u32[]{:S(2)}) async-start(bf16[8,2,192]{2,1,0:T(2,128)(2,1)} %reshape.424), calls=%async_computation | async-start | bytes 16384 | tf_op jit(solution)/shard_map/all_to_all | solution.py:109
  22.9 23.9 %all-to-all-start.1 = ((bf16[8,2,192]{2,1,0:T(2,128)(2,1)}), bf16[8,2,192]{2,1,0:T(2,128)(2,1)S(1)}, u32[]{:S(2)}, u32[]{:S(2)}) async-start(bf16[8,2,192]{2,1,0:T(2,128)(2,1)} %reshape.426), calls=%async_computation.1 | async-start | bytes 16384 | tf_op jit(solution)/shard_map/all_to_all | solution.py:108
  46.8 6.1 copy-start.4
  46.8 24.7 %all-to-all-start.3 = ((bf16[8,2,24576]{2,1,0:T(2,128)(2,1)}), bf16[8,2,24576]{2,1,0:T(2,128)(2,1)}, u32[]{:S(2)}, u32[]{:S(2)}) async-start(bf16[8,2,24576]{2,1,0:T(2,128)(2,1)} %reshape.428), calls=%async_computation.3 | async-start | bytes 1572864 | tf_op jit(solution)/shard_map/all_to_all | solution.py:106
  71.5 48.1 %all-to-all-start.4 = ((bf16[8,2,24576]{2,1,0:T(2,128)(2,1)}), bf16[8,2,24576]{2,1,0:T(2,128)(2,1)S(1)}, u32[]{:S(2)}, u32[]{:S(2)}) async-start(bf16[8,2,24576]{2,1,0:T(2,128)(2,1)} %reshape.422), calls=%async_computation.4 | async-start | bytes 1572864 | tf_op jit(solution)/shard_map/all_to_all | solution.py:105
  77.2 332.6 %all-gather.2.cloned.1.call-start = ((), (), s32[]{:S(2)}) async-start(), calls=%async_computation.8 | async-start | bytes 18874368 | tf_op jit(solution)/shard_map/all_gather | solution.py:127
  119.5 6.2 copy-start.10
  119.5 77.4 %all-to-all-start.2 = ((bf16[8,2,49152]{2,1,0:T(2,128)(2,1)}), bf16[8,2,49152]{2,1,0:T(2,128)(2,1)}, u32[]{:S(2)}, u32[]{:S(2)}) async-start(bf16[8,2,49152]{2,1,0:T(2,128)(2,1)} %reshape.420), calls=%async_computation.2 | async-start | bytes 3145728 | tf_op jit(solution)/shard_map/all_to_all | solution.py:107
  360.1 4.4 copy-start.6
  360.1 39.5 %all-to-all-start.5 = ((bf16[8,2,49152]{2,1,0:T(2,128)(2,1)}), bf16[8,2,49152]{2,1,0:T(2,128)(2,1)}, u32[]{:S(2)}, u32[]{:S(2)}) async-start(bf16[8,2,49152]{2,1,0:T(2,128)(2,1)} %reshape.430), calls=%async_computation.5 | async-start | bytes 3145728 | tf_op jit(solution)/shard_map/all_to_all | solution.py:124
  409.8 8.2 %copy-start.2 = (bf16[1,192,2048]{2,1,0:T(8,128)(2,1)S(1)}, bf16[1,192,2048]{2,1,0:T(8,128)(2,1)}, u32[]{:S(2)}) copy-start(bf16[1,192,2048]{2,1,0:T(8,128)(2,1)} %param.21) | copy-start | bytes 2359300
  409.8 8.3 %copy-start.5 = (f32[2048]{0:T(1024)S(1)}, f32[2048]{0:T(1024)}, u32[]{:S(2)}) copy-start(f32[2048]{0:T(1024)} %param.29) | copy-start | bytes 24580
  418.0 1.2 copy-start.1
  418.0 1.1 copy-start.8
  435.7 121.7 %copy-start.11 = (bf16[1,2048,512]{2,1,0:T(8,128)(2,1)S(1)}, bf16[1,2048,512]{2,1,0:T(8,128)(2,1)}, u32[]{:S(2)}) copy-start(bf16[1,2048,512]{2,1,0:T(8,128)(2,1)} %param.35) | copy-start | bytes 6291460
  555.1 2.3 copy-start.3
  572.4 4.1 copy-start.7
  572.4 121.1 %all-to-all-start.7 = ((bf16[32,36,2048]{2,1,0:T(8,128)(2,1)}), bf16[32,36,2048]{2,1,0:T(8,128)(2,1)}, u32[]{:S(2)}, u32[]{:S(2)}) async-start(bf16[32,36,2048]{2,1,0:T(8,128)(2,1)} %convolution_convert_fusion), calls=%async_computation.7 | async-start | bytes 10485760 | tf_op jit(solution)/shard_map/all_to_all | solution.py:157
  728.8 8.0 %copy-start.9 = (f32[2048]{0:T(1024)S(1)}, f32[2048]{0:T(1024)}, u32[]{:S(2)}) copy-start(f32[2048]{0:T(1024)} %param.31) | copy-start | bytes 24580
Sparse Core Ops, SparseCore 0:
  80.1 262.0 all-gather.1
where the time goes:
time: 758 us; the launch traced here: 748 us
  local copies, waits for them, and re-layouts  207 us (27%)
  waiting for transfers between devices  187 us (25%)
  blocking collectives  119 us (16%)
  other arithmetic  94.6 us (12%)
  matrix products  88.1 us (12%)
  starting transfers between devices  37.6 us (5%)
  between operations  14.2 us (2%)
    all_to_all x1, blocking collectives, local(): lax.all_to_all(outgoing, ('sp', 'dp'), split_axis=0, concat_axis=0, tiled...  119 us
    all_to_all x1, waiting for transfers between devices, local(): lax.all_to_all(expert_out, ('sp', 'dp'), split_axis=0, concat_axis=0, til...  115 us
    unnamed x46, local copies, waits for them, and re-layouts  68 us
    unnamed x9, other arithmetic  63.3 us
    all_to_all x1, waiting for transfers between devices, local(): lax.all_to_all(value_rows, 'sp', split_axis=2, concat_axis=1, tiled=True)  38.3 us
    all_to_all x1, waiting for transfers between devices, local(): lax.all_to_all(normed, 'sp', split_axis=1, concat_axis=2, tiled=True)[0]  28.7 us
    transpose x6, local copies, waits for them, and re-layouts, to_blocks(): return jnp.moveaxis(shaped, 2, 1)  25 us
    dot_general x6, matrix products, cell_block(): jnp.einsum('hls,hsv->hlv', scores, value_part, precision=HIGHEST)  18.1 us
  transfers between devices with their start and end apart: 8, of which 5 were waited for; matrix products, arithmetic and copies ran while one was open for 40% of the time, Pallas kernels for 0%

commit v1 on v0

v1 whole, which is shorter than its diff:
```python
import functools

import jax
import jax.numpy as jnp
from jax import lax
from jax.experimental import pallas as pl
from jax.experimental.pallas import tpu as pltpu
from jax.sharding import PartitionSpec as P

EPSILON = 1e-06
ROUTE_BOOST = 2.5
HIGHEST = lax.Precision.HIGHEST
ROWS_BY_ROWS = (((0,), (0,)), ((), ()))
LANES_BY_LANES = (((1,), (1,)), ((), ()))


def root_norm(values, gains):
    return values * lax.rsqrt(jnp.mean(values * values, axis=-1, keepdims=True) + EPSILON) * gains


def split_parts(values, count):
    parts = []
    for _ in range(count):
        part = lax.reduce_precision(values, 8, 7)
        parts.append(part.astype(jnp.bfloat16))
        values = values - part
    return parts


def kernel_parts(values, count):
    parts = []
    for _ in range(count):
        parts.append(values.astype(jnp.bfloat16))
        values = values - parts[-1].astype(jnp.float32)
    return parts


def mxu(left, right, dims=(((1,), (0,)), ((), ()))):
    return lax.dot_general(left, right, dims, preferred_element_type=jnp.float32)


def column_of(table, head):
    lanes = lax.broadcasted_iota(jnp.int32, table.shape, 1)
    return jnp.sum(jnp.where(lanes == head, table, 0.0), axis=1, keepdims=True)


def write_states(k_ref, v_ref, source_ref, state_ref, normal_ref, *, group, qk, vd):
    for j in range(group):
        head = pl.program_id(0) * group + j
        source = column_of(source_ref[...], head)
        top = jnp.max(source, axis=0, keepdims=True)
        keys = k_ref[:, j * qk : (j + 1) * qk].astype(jnp.float32) * qk ** (-0.5)
        written = jnp.exp(source - top) * keys
        values = v_ref[:, j * vd : (j + 1) * vd]
        state_ref[j] = sum(mxu(part, values, ROWS_BY_ROWS) for part in kernel_parts(written, 3))
        normal_ref[j] = jnp.sum(written, axis=0, keepdims=True)


def chain_states(place_ref, stats_ref, written_ref, prefix_ref, entry_ref, *, steps, mine, heads, qk):
    place = place_ref[0]
    for j in range(mine):
        state = jnp.zeros(written_ref.shape[2:], jnp.float32)
        level = jnp.zeros((1, 1), jnp.float32)
        for t in range(steps):
            prefix_ref[t, j] = state
            row = stats_ref[t, pl.ds(place * mine + j, 1), :]
            top, fall = row[:, qk : qk + 1], row[:, qk + 1 : qk + 2]
            peak = jnp.maximum(level, top)
            state = jnp.exp(level - peak) * state + jnp.exp(top - peak) * written_ref[t, j]
            level = fall + peak
    normal = jnp.zeros((heads, qk), jnp.float32)
    level = jnp.zeros((heads, 1), jnp.float32)
    for t in range(steps):
        table = stats_ref[t, :heads, :]
        top, fall = table[:, qk : qk + 1], table[:, qk + 1 : qk + 2]
        peak = jnp.maximum(level, top)
        grown = jnp.exp(level - peak) * normal + jnp.exp(top - peak) * table[:, :qk]
        normal = jnp.where(t < place, grown, normal)
        level = jnp.where(t < place, fall + peak, level)
    entry_ref[:, :qk] = normal
    entry_ref[:, qk:] = jnp.broadcast_to(level, (heads, entry_ref.shape[1] - qk))


def read_cells(q_ref, k_ref, v_ref, total_ref, row_ref, prefix_ref, entry_ref, gain_ref, out_ref, *, group, qk, vd):
    length = q_ref.shape[0]
    rows = lax.broadcasted_iota(jnp.int32, (length, length), 0)
    lanes = lax.broadcasted_iota(jnp.int32, (length, length), 1)
    for j in range(group):
        head = pl.program_id(0) * group + j
        total = column_of(total_ref[...], head)
        source = jnp.where(lanes <= rows, row_ref[0, j : j + 1, :], -jnp.inf)
        level = entry_ref[0, j : j + 1, qk : qk + 1]
        normal = entry_ref[0, j : j + 1, :qk]
        peak = jnp.maximum(jnp.max(source, axis=1, keepdims=True), level)
        query = q_ref[:, j * qk : (j + 1) * qk]
        values = v_ref[:, j * vd : (j + 1) * vd]
        scores = mxu(query, k_ref[:, j * qk : (j + 1) * qk], LANES_BY_LANES) * qk ** (-0.5)
        scores = scores * jnp.exp(source - peak)
        carried = jnp.exp(level - peak)
        numerator = sum(mxu(part, values) for part in kernel_parts(scores, 3)) + carried * sum(
            mxu(query, part) for part in kernel_parts(prefix_ref[j], 3)
        )
        denominator = jnp.sum(scores, axis=1, keepdims=True) + carried * jnp.sum(
            query.astype(jnp.float32) * normal, axis=1, keepdims=True
        )
        cell = numerator / jnp.maximum(jnp.abs(denominator), jnp.exp(-(total + peak)))
        out_ref[:, j * vd : (j + 1) * vd] = root_norm(cell, gain_ref[0, j : j + 1, :]).astype(jnp.bfloat16)


def cell_rows(queries, key_rows, value_rows, input_gate, forget_gate, head_gain):
    steps = lax.axis_size("sp")
    place = lax.axis_index("sp")
    mine, vd = head_gain.shape
    length, heads = input_gate.shape
    qk = queries.shape[1] // heads
    group = 4 if heads % 4 == 0 else 1
    blocks = heads // group
    decay = jax.nn.log_sigmoid(forget_gate.astype(jnp.float32))
    lower = jnp.tril(jnp.ones((length, length), jnp.float32))
    total = jnp.dot(lower, decay, precision=HIGHEST)
    source = input_gate.astype(jnp.float32) - total

    def lanes_of(width):
        return pl.BlockSpec((length, group * width), lambda i: (0, i))

    table = pl.BlockSpec((length, heads), lambda i: (0, 0))
    written, normals = pl.pallas_call(
        functools.partial(write_states, group=group, qk=qk, vd=vd),
        grid=(blocks,),
        in_specs=[lanes_of(qk), lanes_of(vd), table],
        out_specs=[
            pl.BlockSpec((group, qk, vd), lambda i: (i, 0, 0)),
            pl.BlockSpec((group, 1, qk), lambda i: (i, 0, 0)),
        ],
        out_shape=[
            jax.ShapeDtypeStruct((heads, qk, vd), jnp.float32),
            jax.ShapeDtypeStruct((heads, 1, qk), jnp.float32),
        ],
        name="write_states",
    )(key_rows, value_rows, source)
    stats = jnp.concatenate(
        [
            normals[:, 0],
            jnp.max(source, axis=0)[:, None],
            total[-1][:, None],
            jnp.zeros((heads, vd - qk - 2), jnp.float32),
        ],
        axis=1,
    )
    stats = lax.all_gather(jnp.concatenate([stats, head_gain], axis=0), "sp", axis=0)
    gains = stats[:, heads:].reshape(blocks, group, vd)
    arrived = lax.all_to_all(written.reshape(steps, mine, qk, vd), "sp", split_axis=0, concat_axis=0, tiled=True)
    whole = pl.BlockSpec(memory_space=pltpu.VMEM)
    prefixes, entry = pl.pallas_call(
        functools.partial(chain_states, steps=steps, mine=mine, heads=heads, qk=qk),
        in_specs=[pl.BlockSpec(memory_space=pltpu.SMEM), whole, whole],
        out_specs=[whole, whole],
        out_shape=[
            jax.ShapeDtypeStruct((steps, mine, qk, vd), jnp.float32),
            jax.ShapeDtypeStruct((heads, 2 * qk), jnp.float32),
        ],
        name="chain_states",
    )(place.reshape(1).astype(jnp.int32), stats, arrived)
    prefixes = lax.all_to_all(prefixes, "sp", split_axis=0, concat_axis=0, tiled=True)
    row = pl.BlockSpec((1, group, length), lambda i: (i, 0, 0))
    return pl.pallas_call(
        functools.partial(read_cells, group=group, qk=qk, vd=vd),
        grid=(blocks,),
        in_specs=[
            lanes_of(qk),
            lanes_of(qk),
            lanes_of(vd),
            table,
            row,
            pl.BlockSpec((group, qk, vd), lambda i: (i, 0, 0)),
            pl.BlockSpec((1, group, 2 * qk), lambda i: (i, 0, 0)),
            pl.BlockSpec((1, group, vd), lambda i: (i, 0, 0)),
        ],
        out_specs=lanes_of(vd),
        out_shape=jax.ShapeDtypeStruct((length, heads * vd), jnp.bfloat16),
        name="read_cells",
    )(
        queries,
        key_rows,
        value_rows,
        total,
        source.T.reshape(blocks, group, length),
        prefixes.reshape(heads, qk, vd),
        entry.reshape(blocks, group, 2 * qk),
        gains,
    )


def gather_rows(weight):
    share = weight.shape[0] // lax.axis_size("dp")
    piece = lax.dynamic_slice_in_dim(weight, lax.axis_index("dp") * share, share, 0)
    return lax.all_gather(piece, ("sp", "dp"), axis=0, tiled=True)


def local(
    stream,
    queries,
    key_rows,
    value_rows,
    input_gate,
    forget_gate,
    head_gain,
    out_weight,
    mix_gain,
    ffn_gain,
    final_gain,
    expert_ids,
    route_scores,
    expert_gate,
    expert_up,
    expert_down,
    shared_gate,
    shared_up,
    shared_down,
):
    token_count = stream.shape[1]
    model_width = stream.shape[2]
    gathered_weight = gather_rows(out_weight)
    normed = cell_rows(
        queries[0], key_rows[0], value_rows[0], input_gate[0], forget_gate[0], head_gain
    )
    mixer_out = jnp.dot(normed, gathered_weight, preferred_element_type=jnp.float32)
    residual = stream[0].astype(jnp.float32) + root_norm(mixer_out, mix_gain)
    ffn_input = root_norm(residual, ffn_gain).astype(jnp.bfloat16)
    top_count = expert_ids.shape[2]
    local_count = expert_gate.shape[0]
    expert_count = lax.axis_size("sp") * lax.axis_size("dp") * local_count
    capacity = max(2, 3 * token_count * top_count // (2 * expert_count))
    capacity = -(-capacity // 8) * 8
    ids = expert_ids[0]
    named = ids[:, :, None] == jnp.arange(expert_count, dtype=jnp.int32)[None, None, :]
    chosen = jnp.any(named, axis=1).astype(jnp.bfloat16)
    earlier = jnp.tril(jnp.ones((token_count, token_count), jnp.bfloat16), -1)
    rank = jnp.dot(earlier, chosen, preferred_element_type=jnp.float32).astype(jnp.int32)
    before = jnp.sum(jnp.where(named, rank[:, None, :], 0), axis=2)
    slot_index = ids * capacity + before
    slots = jnp.arange(expert_count * capacity, dtype=jnp.int32)[None, :]
    scores = route_scores[0]
    route_share = scores / jnp.sum(scores, axis=1, keepdims=True) * ROUTE_BOOST
    placed = jnp.zeros((token_count, expert_count * capacity), jnp.bfloat16)
    shares = jnp.zeros((token_count, expert_count * capacity), jnp.float32)
    for column in range(top_count):
        hit = slot_index[:, column][:, None] == slots
        placed = jnp.where(hit, jnp.ones((), jnp.bfloat16), placed)
        shares = jnp.where(hit, route_share[:, column][:, None], shares)
    share_high, share_low = split_parts(shares, 2)
    outgoing = mxu(placed, ffn_input, ROWS_BY_ROWS).astype(jnp.bfloat16)
    outgoing = outgoing.reshape(expert_count, capacity, model_width)
    slot_rows = lax.all_to_all(outgoing, ("sp", "dp"), split_axis=0, concat_axis=0, tiled=True)
    shaped = slot_rows.reshape(-1, local_count, slot_rows.shape[1], model_width)
    gate_proj = jnp.einsum(
        "nlcd,ldf->nlcf", shaped, expert_gate, preferred_element_type=jnp.float32
    )
    up_proj = jnp.einsum("nlcd,ldf->nlcf", shaped, expert_up, preferred_element_type=jnp.float32)
    hidden = (jax.nn.silu(gate_proj) * up_proj).astype(jnp.bfloat16)
    answer = jnp.einsum("nlcf,lfd->nlcd", hidden, expert_down, preferred_element_type=jnp.float32)
    expert_out = answer.astype(jnp.bfloat16).reshape(slot_rows.shape)
    returned = lax.all_to_all(expert_out, ("sp", "dp"), split_axis=0, concat_axis=0, tiled=True)
    answers = returned.reshape(expert_count * capacity, model_width)
    shared_hidden = (
        jax.nn.silu(jnp.dot(ffn_input, shared_gate, preferred_element_type=jnp.float32))
        * jnp.dot(ffn_input, shared_up, preferred_element_type=jnp.float32)
    ).astype(jnp.bfloat16)
    shared_out = jnp.dot(shared_hidden, shared_down, preferred_element_type=jnp.float32)
    moe_total = mxu(share_high, answers) + mxu(share_low, answers) + shared_out
    result = (residual + root_norm(moe_total, final_gain)).astype(jnp.bfloat16)
    return result[None]


def solution(mesh):
    placed = (
        P("dp", "sp", None),
        P("dp", "sp", None),
        P("dp", "sp", None),
        P("dp", "sp", None),
        P("dp", "sp", None),
        P("dp", "sp", None),
        P("sp", None),
        P("sp", None),
        P(),
        P(),
        P(),
        P("dp", "sp", None),
        P("dp", "sp", None),
        P(("sp", "dp"), None, None),
        P(("sp", "dp"), None, None),
        P(("sp", "dp"), None, None),
        P(),
        P(),
        P(),
    )
    return jax.shard_map(
        local, mesh=mesh, in_specs=placed, out_specs=P("dp", "sp", None), check_vma=False
    )
```

time: 758 us -> 507 us (0.67); the launches traced: 748 us -> 506 us
  local copies, waits for them, and re-layouts: 207 us -> 9.52 us
  blocking collectives: 119 us -> 222 us
  other arithmetic: 94.6 us -> 5.38 us
  matrix products: 88.1 us -> 40.6 us
  starting transfers between devices: 37.6 us -> 15.7 us
  Pallas kernels: 0 us -> 17.2 us
    all_gather x0 -> x1, blocking collectives: none -> 102 us  [cell_rows(): lax.all_gather(jnp.concatenate([stats, head_gain], axis=0), 'sp', axis=0)]
    unnamed x46 -> x39, local copies, waits for them, and re-layouts: 68 us -> 4.43 us
    unnamed x9 -> x1, other arithmetic: 63.3 us -> 0.08 us
    dot_general x31 -> x6, matrix products: 63 us -> 20.7 us  [the longest x3 11.3 us: mxu(): lax.dot_general(left, right, dims, preferred_element_type=jnp.float32)]
    transpose x7 -> x1, local copies, waits for them, and re-layouts: 31.1 us -> 0.06 us  [cell_rows(): source.T.reshape(blocks, group, length)]
    gather x3 -> x0, local copies, waits for them, and re-layouts: 23.2 us -> none  [the longest x2 13.2 us: local(): ffn_input[source]]
    all_to_all x6 -> x2, starting transfers between devices: 33 us -> 11.9 us  [the longest x1 7.43 us: cell_rows(): lax.all_to_all(written.reshape(steps, mine, qk, vd), 'sp', split_axis=0,...]
    mul x6 -> x0, local copies, waits for them, and re-layouts: 17.8 us -> none  [the longest x2 8.82 us: root_norm(): values * lax.rsqrt(jnp.mean(values * values, axis=-1, keepdims=True) + EP...]
  transfers between devices with their start and end apart: 8 -> 4, of which waited for: 5 -> 2; matrix products, arithmetic and copies ran while one was open for 40% -> 1% of each run, Pallas kernels for 0% -> 3%
where the time goes in v1:
time: 507 us; the launch traced here: 506 us
  blocking collectives  222 us (44%)
  waiting for transfers between devices  182 us (36%)
  matrix products  40.6 us (8%)
  Pallas kernels  17.2 us (3%)
  starting transfers between devices  15.7 us (3%)
  between operations  13.7 us (3%)
  local copies, waits for them, and re-layouts  9.52 us (2%)
  other arithmetic  5.38 us (1%)
    all_to_all x1, blocking collectives, local(): lax.all_to_all(outgoing, ('sp', 'dp'), split_axis=0, concat_axis=0, tiled...  120 us
    all_to_all x1, waiting for transfers between devices, local(): lax.all_to_all(expert_out, ('sp', 'dp'), split_axis=0, concat_axis=0, til...  116 us
    all_gather x1, blocking collectives, cell_rows(): lax.all_gather(jnp.concatenate([stats, head_gain], axis=0), 'sp', axis=0)  102 us
    all_to_all x1, waiting for transfers between devices, cell_rows(): lax.all_to_all(prefixes, 'sp', split_axis=0, concat_axis=0, tiled=True)  65.8 us
    dot_general x3, matrix products, mxu(): lax.dot_general(left, right, dims, preferred_element_type=jnp.float32)  11.3 us
    dot_general x1, matrix products, local(): jnp.einsum('nlcf,lfd->nlcd', hidden, expert_down, preferred_element_type=...  10.6 us
  transfers between devices with their start and end apart: 4, of which 2 were waited for; matrix products, arithmetic and copies ran while one was open for 1% of the time, Pallas kernels for 3%

profile of v1, /device:TPU:0, one launch (start us, length us, event | category | flops | bytes accessed | tf_op | source)
XLA Modules:
  0.0 506.3 jit_solution(17335351768121548337)
XLA Ops:
  6.5 0.0 copy-start
  6.5 0.0 all-gather.4.cloned.1.call-start
  6.5 2.0 constant_dynamic-slice_fusion
  8.6 0.0 all-gather.4.cloned.1.call-update
  8.6 0.9 fusion.60
  9.5 0.1 copy.49.total_ref
  9.7 0.0 copy-start.9
  9.7 0.8 copy.44
  10.5 0.7 fusion.93
  11.2 5.3 %write_states.1 = (f32[16,128,256]{2,1,0:T(8,128)}, f32[16,1,128]{2,1,0:T(1,128)}) custom-call(bf16[192,2048]{1,0:T(8,128)(2,1)} %bitcast.136, bf16[192,4096]{1,0:T(8,128)(2,1)} %bitcast.133, f32[192,16]{1,0:T(8,128)} %get-tuple-element.14.source_ref), custom_call_target="tpu_custom_call" | custom-call | tf_op jit(solution)/shard_map/write_states/pallas_call | solution.py:127
  16.5 0.0 copy-done.9
  16.5 7.4 %all-to-all-start = ((f32[8,2,128,256]{3,2,1,0:T(8,128)}), f32[8,2,128,256]{3,2,1,0:T(8,128)}, u32[]{:S(2)}, u32[]{:S(2)}) async-start(f32[8,2,128,256]{3,2,1,0:T(8,128)} %bitcast.138), calls=%async_computation | async-start | bytes 4194304 | tf_op jit(solution)/shard_map/all_to_all | solution.py:152
  23.9 0.1 copy.47
  24.0 0.1 slice_bitcast_fusion
  24.1 0.0 copy-done.16
  24.1 0.0 copy-done.17
  24.1 0.1 maximum_bitcast_fusion
  24.1 102.4 %all-gather.1.stats_ref = f32[8,18,256]{2,1,0:T(8,128)} all-gather(f32[1,18,256]{2,1,0:T(8,128)S(1)} %maximum_bitcast_fusion), channel_id=2, replica_groups=mesh['sp'=8,'dp'=4] {'sp'}, dimensions={0}, use_global_device_ids=true | all-gather | bytes 165888 | tf_op jit(solution)/shard_map/all_gather | solution.py:150
  126.6 0.0 all-to-all-done.written_ref
  126.6 3.5 chain_states.1
  130.1 4.5 all-to-all-start.1
  134.6 0.8 slice.41
  135.4 0.6 reshape.87.gain_ref
  136.0 0.0 copy-done.8
  136.0 0.1 copy.46
  136.1 0.6 reshape.82.row_ref
  136.7 0.0 copy-done.11
  136.7 0.2 convolution_convert_fusion.2
  137.0 0.1 select_reduce_fusion
  137.0 0.0 copy-done.12
  137.1 0.6 reshape.86.entry_ref
  137.7 65.8 %all-to-all-done.1 = f32[8,2,128,256]{3,2,1,0:T(8,128)} async-done(((f32[8,2,128,256]{3,2,1,0:T(8,128)}), f32[8,2,128,256]{3,2,1,0:T(8,128)}, u32[]{:S(2)}, u32[]{:S(2)}) %all-to-all-start.1) | async-done | bytes 2097184 | tf_op jit(solution)/shard_map/all_to_all | solution.py:164
  203.4 8.4 %read_cells.1 = bf16[192,4096]{1,0:T(8,128)(2,1)} custom-call(bf16[192,2048]{1,0:T(8,128)(2,1)} %bitcast.140, bf16[192,2048]{1,0:T(8,128)(2,1)} %bitcast.137, bf16[192,4096]{1,0:T(8,128)(2,1)} %bitcast.134, f32[192,16]{1,0:T(8,128)} %copy-done.9, f32[4,4,192]{2,1,0:T(4,128)} %reshape.82.row_ref, f32[16,128,256]{2,1,0:T(8,128)} %bitcast.13.prefix_ref, ...), custom_call_target="tpu_custom_call" | custom-call | tf_op jit(solution)/shard_map/read_cells/pallas_call | solution.py:166
  211.9 0.0 all-gather.4.cloned.1.call-done
  211.9 8.2 %multiply_reduce_fusion.2 = (f32[192]{0:T(256)S(1)}, f32[192,2048]{1,0:T(8,128)S(1)}) fusion(bf16[192,4096]{1,0:T(8,128)(2,1)} %read_cells.1, bf16[4096,2048]{1,0:T(8,128)(2,1)} %all-gather.4.cloned.1.call-done), kind=kOutput, calls=%fused_computation.21 | convolution fusion | flops 3222011648 | bytes 19923712 | tf_op jit(solution)/shard_map/dot_general | solution.py:227
  220.1 0.0 copy-start.2
  220.1 0.0 copy-start.4
  220.2 0.0 copy-start.14
  220.2 0.0 copy-done.3
  220.2 0.0 copy-done.10
  220.2 0.5 multiply_reduce_fusion.1
  220.7 1.2 copy-done.4
  221.8 0.0 copy-done.14
  221.9 0.4 multiply_convert_fusion
  222.3 0.0 copy-done.2
  222.3 1.8 convolution_convert_fusion
  224.1 0.0 copy-start.18
  224.2 119.5 %all_to_all.20 = bf16[32,40,2048]{2,1,0:T(8,128)(2,1)S(1)} all-to-all(bf16[32,40,2048]{2,1,0:T(8,128)(2,1)S(1)} %bitcast.135), channel_id=1, replica_groups=mesh['sp'=8,'dp'=4] {'sp','dp'}, dimensions={0} | all-to-all | bytes 10485760 | tf_op jit(solution)/shard_map/all_to_all | solution.py:254
  343.7 2.3 copy-done.5
  346.0 0.0 copy-done.18
  346.0 4.5 fusion.5
  350.6 0.0 copy-done
  350.6 10.6 %convolution_convert_fusion.1 = bf16[32,40,2048]{2,1,0:T(8,128)(2,1)} fusion(bf16[1,512,2048]{2,1,0:T(8,128)(2,1)S(1)} %copy-done, f32[32,40,512]{2,1,0:T(8,128)} %fusion.5, bf16[32,40,2048]{2,1,0:T(8,128)(2,1)} %copy-done.5, bf16[1,2048,512]{2,1,0:T(8,128)(2,1)} %param.32), kind=kOutput, calls=%fused_computation.1 | convolution fusion | flops 5375262720 | bytes 17301504 | tf_op jit(solution)/shard_map/nlcf,lfd->nlcd/dot_general | solution.py:261
  361.1 3.8 all-to-all-start.3
  364.9 0.0 copy-done.13
  365.0 0.0 copy-done.7
  365.0 0.6 fusion.96
  365.6 116.4 %all-to-all-done.3 = bf16[32,40,2048]{2,1,0:T(8,128)(2,1)} async-done(((bf16[32,40,2048]{2,1,0:T(8,128)(2,1)}), bf16[32,40,2048]{2,1,0:T(8,128)(2,1)}, u32[]{:S(2)}, u32[]{:S(2)}) %all-to-all-start.3) | async-done | bytes 5242912 | tf_op jit(solution)/shard_map/all_to_all | solution.py:263
  481.9 4.0 fusion.25
  486.0 0.0 copy-start.6
  486.0 5.5 %convolution_add_fusion.1 = f32[192,2048]{1,0:T(8,128)} fusion(f32[192,2048]{1,0:T(8,128)S(1)} %fusion.25, bf16[1280,2048]{1,0:T(8,128)(2,1)} %bitcast.40, f32[192]{0:T(256)S(1)} %bitcast.160, s32[192]{0:T(256)S(1)} %bitcast.150, f32[192]{0:T(256)S(1)} %bitcast.162, s32[192]{0:T(256)S(1)} %bitcast.153, f32[192]{0:T(256)S(1)} %bitcast.164, ...), kind=kOutput, calls=%fused_computation.10 | convolution fusion | flops 1009975296 | bytes 8394752 | tf_op jit(solution)/shard_map/dot_general | solution.py:39
  491.5 0.0 copy-done.6
  491.5 4.3 multiply_reduce_fusion
  495.8 3.6 fusion.21
  (25 shorter events, 0.1 us)
Async XLA Ops:
  6.5 344.0 %copy-start = (bf16[1,512,2048]{2,1,0:T(8,128)(2,1)S(1)}, bf16[1,512,2048]{2,1,0:T(8,128)(2,1)}, u32[]{:S(2)}) copy-start(bf16[1,512,2048]{2,1,0:T(8,128)(2,1)} %param.34) | copy-start | bytes 6291460
  6.5 205.4 %all-gather.4.cloned.1.call-start = ((), (), s32[]{:S(2)}) async-start(), calls=%async_computation.4 | async-start | bytes 17301504 | tf_op jit(solution)/shard_map/all_gather | solution.py:197
  9.7 6.8 %copy-start.9 = (f32[192,16]{1,0:T(8,128)}, f32[192,16]{1,0:T(8,128)S(1)}, u32[]{:S(2)}) copy-start(f32[192,16]{1,0:T(8,128)S(1)} %copy.49.total_ref) | copy-start | bytes 36868
  16.4 7.6 %copy-start.16 = (f32[16,1,128]{2,1,0:T(1,128)S(1)}, f32[16,1,128]{2,1,0:T(1,128)}, u32[]{:S(2)}) copy-start(f32[16,1,128]{2,1,0:T(1,128)} %get-tuple-element.9) | copy-start | bytes 24580
  16.5 7.6 %copy-start.17 = (f32[2,256]{1,0:T(2,128)S(1)}, f32[2,256]{1,0:T(2,128)}, u32[]{:S(2)}) copy-start(f32[2,256]{1,0:T(2,128)} %param.25) | copy-start | bytes 6148
  16.5 110.1 %all-to-all-start = ((f32[8,2,128,256]{3,2,1,0:T(8,128)}), f32[8,2,128,256]{3,2,1,0:T(8,128)}, u32[]{:S(2)}, u32[]{:S(2)}) async-start(f32[8,2,128,256]{3,2,1,0:T(8,128)} %bitcast.138), calls=%async_computation | async-start | bytes 4194304 | tf_op jit(solution)/shard_map/all_to_all | solution.py:152
  130.0 6.0 %copy-start.8 = (f32[192,16]{1,0:T(8,128)S(1)}, f32[192,16]{1,0:T(8,128)}, u32[]{:S(2)}) copy-start(f32[192,16]{1,0:T(8,128)} %get-tuple-element.14.source_ref) | copy-start | bytes 36868
  130.0 6.7 %copy-start.11 = (s32[1,192,4]{1,2,0:T(4,128)S(1)}, s32[1,192,4]{1,2,0:T(4,128)}, u32[]{:S(2)}) copy-start(s32[1,192,4]{1,2,0:T(4,128)} %param.30) | copy-start | bytes 9220
  130.0 7.0 %copy-start.12 = (f32[16,256]{1,0:T(8,128)S(1)}, f32[16,256]{1,0:T(8,128)}, u32[]{:S(2)}) copy-start(f32[16,256]{1,0:T(8,128)} %get-tuple-element.12) | copy-start | bytes 49156
  130.1 73.4 %all-to-all-start.1 = ((f32[8,2,128,256]{3,2,1,0:T(8,128)}), f32[8,2,128,256]{3,2,1,0:T(8,128)}, u32[]{:S(2)}, u32[]{:S(2)}) async-start(f32[8,2,128,256]{3,2,1,0:T(8,128)} %get-tuple-element.11), calls=%async_computation.1 | async-start | bytes 4194304 | tf_op jit(solution)/shard_map/all_to_all | solution.py:164
  211.9 8.3 %copy-start.3 = (bf16[1,192,2048]{2,1,0:T(8,128)(2,1)S(1)}, bf16[1,192,2048]{2,1,0:T(8,128)(2,1)}, u32[]{:S(2)}) copy-start(bf16[1,192,2048]{2,1,0:T(8,128)(2,1)} %param.19) | copy-start | bytes 2359300
  211.9 8.3 %copy-start.10 = (f32[2048]{0:T(1024)S(1)}, f32[2048]{0:T(1024)}, u32[]{:S(2)}) copy-start(f32[2048]{0:T(1024)} %param.27) | copy-start | bytes 24580
  220.1 2.2 copy-start.2
  220.1 1.7 copy-start.4
  220.2 1.7 copy-start.14
  224.1 121.9 %copy-start.18 = (bf16[1,2048,512]{2,1,0:T(8,128)(2,1)S(1)}, bf16[1,2048,512]{2,1,0:T(8,128)(2,1)}, u32[]{:S(2)}) copy-start(bf16[1,2048,512]{2,1,0:T(8,128)(2,1)} %param.33) | copy-start | bytes 6291460
  343.7 2.3 copy-start.5
  361.1 3.8 copy-start.13
  361.1 3.9 copy-start.7
  361.1 120.8 %all-to-all-start.3 = ((bf16[32,40,2048]{2,1,0:T(8,128)(2,1)}), bf16[32,40,2048]{2,1,0:T(8,128)(2,1)}, u32[]{:S(2)}, u32[]{:S(2)}) async-start(bf16[32,40,2048]{2,1,0:T(8,128)(2,1)} %convolution_convert_fusion.1), calls=%async_computation.3 | async-start | bytes 10485760 | tf_op jit(solution)/shard_map/all_to_all | solution.py:263
  486.0 5.5 %copy-start.6 = (bf16[512,2048]{1,0:T(8,128)(2,1)S(1)}, bf16[512,2048]{1,0:T(8,128)(2,1)}, u32[]{:S(2)}) copy-start(bf16[512,2048]{1,0:T(8,128)(2,1)} %param.37) | copy-start | bytes 6291460
  491.5 4.3 copy-start.15
  495.8 3.6 copy-start.1
Sparse Core Ops, SparseCore 0:
  10.2 189.8 all-gather.3
